TPU v7x, 32 devices: a whole 2x2x4 slice. The times are simulated.
32 devices in a mesh: fs: 4 (over z), rep: 4 (over y, x), tp: 2 (over core).
Axes of the slice: x: 2, y: 2, z: 4, core: 2. Of those that a mesh axis runs over, the one named last changes fastest.
Arguments:
- normed_in: bfloat16 [24576, 2048], P(('fs', 'rep')), may hold values from -6 to 6
- cotan_rec: bfloat16 [24576, 2048], P(('fs', 'rep'), 'tp'), may hold values from -0.0390625 to 0.0390625
- cotan_gate: bfloat16 [24576, 2048], P(('fs', 'rep'), 'tp'), may hold values from -0.0390625 to 0.0390625
- factor_rec: bfloat16 [2048, 512], P('fs'), may hold values from -0.125 to 0.125
- factor_gate: bfloat16 [2048, 512], P('fs'), may hold values from -0.125 to 0.125
- first_rec: float32 [512, 2048], P('fs', 'tp'), may hold values from -6 to 6
- first_gate: float32 [512, 2048], P('fs', 'tp'), may hold values from -6 to 6
- second_rec: float32 [512, 2048], P('fs', 'tp'), may hold values from 0.25 to 4
- second_gate: float32 [512, 2048], P('fs', 'tp'), may hold values from 0.25 to 4
- master_rec: float32 [2048, 2048], P('fs', 'tp'), may hold values from -0.125 to 0.125
- master_gate: float32 [2048, 2048], P('fs', 'tp'), may hold values from -0.125 to 0.125
Outputs:
- update_rec: float32 [2048, 2048], P('fs', 'tp')
- update_gate: float32 [2048, 2048], P('fs', 'tp')
- new_first_rec: float32 [512, 2048], P('fs', 'tp')
- new_first_gate: float32 [512, 2048], P('fs', 'tp')
- new_second_rec: float32 [512, 2048], P('fs', 'tp')
- new_second_gate: float32 [512, 2048], P('fs', 'tp')
- copy_rec: bfloat16 [2048, 2048], P(None, 'tp')
- copy_gate: bfloat16 [2048, 2048], P(None, 'tp')
All inputs are finite; a program needn't handle non-finite values.
Results may differ from a plain program's by a relative error of at most 0.007.
Values may be sent and summed in bfloat16 or wider, within the bound.
A program may use at most 128 MiB of HBM per device.

v0:
```python
import jax
import jax.numpy as jnp
from jax import lax
from jax.sharding import PartitionSpec as P

DR = 2048
RANK = 512
beta_first = 0.8
beta_second = 0.9
scale_floor = 0.25
step_rate = 0.01


def split_product(projected, cotan):
    upper = projected.astype(jnp.bfloat16)
    lower = (projected - upper.astype(jnp.float32)).astype(jnp.bfloat16)
    dims = (((0,), (0,)), ((), ()))
    return lax.dot_general(
        upper, cotan, dims, preferred_element_type=jnp.float32
    ) + lax.dot_general(lower, cotan, dims, preferred_element_type=jnp.float32)


def moments(low, first, second):
    new_first = beta_first * first + (1.0 - beta_first) * low
    new_second = beta_second * second + (1.0 - beta_second) * low * low
    return (new_first, new_second, new_first / jnp.sqrt(new_second))


def body(
    normed_in,
    cotan_rec,
    cotan_gate,
    factor_rec,
    factor_gate,
    first_rec,
    first_gate,
    second_rec,
    second_gate,
    master_rec,
    master_gate,
):
    wide_rec = factor_rec.astype(jnp.float32)
    wide_gate = factor_gate.astype(jnp.float32)
    pieces = (
        lax.all_gather(factor_rec, "fs", axis=0, tiled=True),
        lax.all_gather(factor_gate, "fs", axis=0, tiled=True),
    )
    proj_rec = jnp.dot(normed_in, pieces[0], preferred_element_type=jnp.float32)
    proj_gate = jnp.dot(normed_in, pieces[1], preferred_element_type=jnp.float32)
    part_rec = split_product(proj_rec, cotan_rec)
    part_gate = split_product(proj_gate, cotan_gate)
    low_rec, low_gate = (
        lax.psum_scatter(
            part_rec.astype(jnp.bfloat16), "fs", scatter_dimension=0, tiled=True
        ).astype(jnp.float32),
        lax.psum_scatter(
            part_gate.astype(jnp.bfloat16), "fs", scatter_dimension=0, tiled=True
        ).astype(jnp.float32),
    )
    low_rec, low_gate = (
        lax.psum(low_rec.astype(jnp.bfloat16), "rep").astype(jnp.float32),
        lax.psum(low_gate.astype(jnp.bfloat16), "rep").astype(jnp.float32),
    )
    first_r, second_r, direc_rec = moments(low_rec, first_rec, second_rec)
    first_g, second_g, direc_gate = moments(low_gate, first_gate, second_gate)
    total_rec, total_gate = lax.psum(
        (jnp.sum(direc_rec * direc_rec), jnp.sum(direc_gate * direc_gate)), ("fs", "tp")
    )
    entries = float(RANK * DR)
    scale_rec = 1.0 / jnp.sqrt(total_rec / entries + scale_floor)
    scale_gate = 1.0 / jnp.sqrt(total_gate / entries + scale_floor)
    pieces = (
        lax.all_gather(direc_rec, "fs", axis=0, tiled=True),
        lax.all_gather(direc_gate, "fs", axis=0, tiled=True),
    )
    upd_rec = jnp.dot(wide_rec, pieces[0], precision=lax.Precision.HIGHEST)
    upd_gate = jnp.dot(wide_gate, pieces[1], precision=lax.Precision.HIGHEST)
    upd_rec = upd_rec * scale_rec
    upd_gate = upd_gate * scale_gate
    copy_rec = (master_rec - step_rate * upd_rec).astype(jnp.bfloat16)
    copy_gate = (master_gate - step_rate * upd_gate).astype(jnp.bfloat16)
    whole_rec, whole_gate = (
        lax.all_gather(copy_rec, "fs", axis=0, tiled=True),
        lax.all_gather(copy_gate, "fs", axis=0, tiled=True),
    )
    return (upd_rec, upd_gate, first_r, first_g, second_r, second_g, whole_rec, whole_gate)


def solution(mesh):
    return jax.shard_map(
        body,
        mesh=mesh,
        in_specs=(
            P(("fs", "rep"), None),
            P(("fs", "rep"), "tp"),
            P(("fs", "rep"), "tp"),
            P("fs", None),
            P("fs", None),
            P("fs", "tp"),
            P("fs", "tp"),
            P("fs", "tp"),
            P("fs", "tp"),
            P("fs", "tp"),
            P("fs", "tp"),
        ),
        out_specs=(
            P("fs", "tp"),
            P("fs", "tp"),
            P("fs", "tp"),
            P("fs", "tp"),
            P("fs", "tp"),
            P("fs", "tp"),
            P(None, "tp"),
            P(None, "tp"),
        ),
        check_vma=False,
    )
```

profile of v0, /device:TPU:0, one launch (start us, length us, event | category | flops | bytes accessed | tf_op | source)
XLA Modules:
  0.0 479.8 jit_solution(12746524796464819024)
XLA Ops:
  7.2 0.0 copy-start
  7.2 0.0 all-gather.7.cloned.1.call-start
  7.2 0.7 all-gather.7.cloned.1.call-update
  7.9 0.0 all-gather.11.cloned.1.call-start
  8.0 0.7 all-gather.11.cloned.1.call-update
  8.7 0.0 reduce-scatter.3.cloned.1.call-start
  8.7 49.3 %all-gather.7.cloned.1.call-done = bf16[2048,512]{1,0:T(8,128)(2,1)} async-done(((bf16[512,512]{1,0:T(8,128)(2,1)}), bf16[2048,512]{1,0:T(8,128)(2,1)}) %all-gather.7.cloned.1.call-update) | async-done | bytes 2097168 | tf_op jit(solution)/shard_map/all_gather | solution.py:45
  58.0 6.1 %fusion.14 = f32[1536,512]{1,0:T(8,128)S(1)} fusion(bf16[1536,2048]{1,0:T(8,128)(2,1)} %param.11, bf16[2048,512]{1,0:T(8,128)(2,1)} %all-gather.7.cloned.1.call-done), kind=kOutput, calls=%fused_computation.26 | convolution fusion | flops 3221225472 | bytes 11534336 | tf_op jit(solution)/shard_map/dot_general | solution.py:48
  64.1 1.9 fusion
  66.0 2.9 add_convert_fusion.1
  68.9 0.0 reduce-scatter.3.cloned.1.call-update
  68.9 0.0 reduce-scatter.5.cloned.1.call-start
  69.0 35.1 %all-gather.11.cloned.1.call-done = bf16[2048,512]{1,0:T(8,128)(2,1)} async-done(((bf16[512,512]{1,0:T(8,128)(2,1)}), bf16[2048,512]{1,0:T(8,128)(2,1)}) %all-gather.11.cloned.1.call-update) | async-done | bytes 2097168 | tf_op jit(solution)/shard_map/all_gather | solution.py:46
  104.0 6.1 %fusion.15 = f32[1536,512]{1,0:T(8,128)S(1)} fusion(bf16[1536,2048]{1,0:T(8,128)(2,1)} %param.11, bf16[2048,512]{1,0:T(8,128)(2,1)} %all-gather.11.cloned.1.call-done), kind=kOutput, calls=%fused_computation.27 | convolution fusion | flops 3221225472 | bytes 11534336 | tf_op jit(solution)/shard_map/dot_general | solution.py:49
  110.2 1.9 fusion.1
  112.1 2.9 add_convert_fusion
  114.9 0.0 reduce-scatter.5.cloned.1.call-update
  115.0 0.0 copy-start.6
  115.0 0.0 all-reduce.4.cloned.1.call-start
  115.0 18.0 %reduce-scatter.3.cloned.1.call-done = bf16[128,1024]{1,0:T(8,128)(2,1)} async-done(((bf16[512,1024]{1,0:T(8,128)(2,1)}), bf16[128,1024]{1,0:T(8,128)(2,1)}) %reduce-scatter.3.cloned.1.call-update) | async-done | bytes 262160 | tf_op jit(solution)/shard_map/reduce_scatter | solution.py:53
  133.0 28.6 %reduce-scatter.5.cloned.1.call-done = bf16[128,1024]{1,0:T(8,128)(2,1)} async-done(((bf16[512,1024]{1,0:T(8,128)(2,1)}), bf16[128,1024]{1,0:T(8,128)(2,1)}) %reduce-scatter.5.cloned.1.call-update) | async-done | bytes 262160 | tf_op jit(solution)/shard_map/reduce_scatter | solution.py:56
  161.6 0.0 all-reduce.4.cloned.1.call-update
  161.6 0.0 all-gather.9.cloned.1.call-start
  161.7 46.7 %all-reduce.4.cloned.1.call-done = (bf16[128,1024]{1,0:T(8,128)(2,1)}, bf16[128,1024]{1,0:T(8,128)(2,1)}) async-done(((bf16[128,1024]{1,0:T(8,128)(2,1)}, bf16[128,1024]{1,0:T(8,128)(2,1)}), (bf16[128,1024]{1,0:T(8,128)(2,1)}, bf16[128,1024]{1,0:T(8,128)(2,1)})) %all-reduce.4.cloned.1.call-update) | async-done | bytes 524304 | tf_op jit(solution)/shard_map/psum | solution.py:61
  208.4 3.2 multiply_reduce_fusion.1
  211.5 0.0 all-gather.9.cloned.1.call-update
  211.6 0.0 all-gather.13.cloned.1.call-start
  211.6 1.9 multiply_reduce_fusion
  213.5 0.0 all-gather.13.cloned.1.call-update
  213.6 0.0 copy-start.3
  213.6 0.0 all-gather.15.cloned.1.call-start
  213.6 0.1 copy-done.5
  213.7 1.8 copy.19
  215.5 17.6 %all-reduce = (f32[]{:T(128)}, f32[]{:T(128)}) all-reduce(f32[]{:T(128)} %get-tuple-element.24, f32[]{:T(128)} %get-tuple-element.20), channel_id=1, replica_groups=mesh['fs'=4,'rep'=4,'tp'=2] {'fs','tp'}, use_global_device_ids=true, to_apply=%region_3.0 | all-reduce | flops 2 | bytes 16 | tf_op jit(solution)/shard_map/psum | solution.py:66
  233.8 23.8 %all-gather.9.cloned.1.call-done = f32[512,1024]{1,0:T(8,128)} async-done(((f32[128,1024]{1,0:T(8,128)}), f32[512,1024]{1,0:T(8,128)}) %all-gather.9.cloned.1.call-update) | async-done | bytes 2097168 | tf_op jit(solution)/shard_map/all_gather | solution.py:73
  257.6 6.7 %subtract_convert_fusion.3 = (bf16[512,1024]{0,1:T(8,128)(2,1)}, f32[512,1024]{0,1:T(8,128)S(1)}) fusion(f32[512,1024]{0,1:T(8,128)} %copy.19, f32[]{:T(128)S(6)} %sqrt.13, f32[512,1024]{1,0:T(8,128)} %all-gather.9.cloned.1.call-done, bf16[512,512]{1,0:T(8,128)(2,1)S(1)} %copy-done.3), kind=kOutput, calls=%fused_computation.3 | convolution fusion | flops 3223322624 | bytes 7864324 | tf_op jit(solution)/shard_map/dot_general | solution.py:76
  264.3 0.0 all-gather.15.cloned.1.call-update
  264.3 0.0 all-gather.17.cloned.1.call-start
  264.4 3.0 copy.20
  268.1 36.1 %all-gather.13.cloned.1.call-done = f32[512,1024]{1,0:T(8,128)} async-done(((f32[128,1024]{1,0:T(8,128)}), f32[512,1024]{1,0:T(8,128)}) %all-gather.13.cloned.1.call-update) | async-done | bytes 2097168 | tf_op jit(solution)/shard_map/all_gather | solution.py:74
  304.2 7.5 %subtract_convert_fusion.2 = (bf16[512,1024]{0,1:T(8,128)(2,1)}, f32[512,1024]{0,1:T(8,128)}) fusion(f32[512,1024]{0,1:T(8,128)} %copy.20, f32[]{:T(128)S(6)} %sqrt.15, f32[512,1024]{1,0:T(8,128)} %all-gather.13.cloned.1.call-done, bf16[512,512]{1,0:T(8,128)(2,1)S(1)} %copy-done.4), kind=kOutput, calls=%fused_computation.2 | convolution fusion | flops 3223322624 | bytes 7864324 | tf_op jit(solution)/shard_map/dot_general | solution.py:77
  311.7 0.0 all-gather.17.cloned.1.call-update
  311.7 1.8 copy.21
  313.5 3.0 copy.22
  316.5 69.5 %all-gather.15.cloned.1.call-done = bf16[2048,1024]{0,1:T(8,128)(2,1)} async-done(((bf16[512,1024]{0,1:T(8,128)(2,1)}), bf16[2048,1024]{0,1:T(8,128)(2,1)}) %all-gather.15.cloned.1.call-update) | async-done | bytes 4194320 | tf_op jit(solution)/shard_map/all_gather | solution.py:83
  385.9 6.4 %copy.23 = bf16[2048,1024]{1,0:T(8,128)(2,1)} copy(bf16[2048,1024]{0,1:T(8,128)(2,1)} %all-gather.15.cloned.1.call-done) | data formatting | bytes 8388608
  392.3 74.4 %all-gather.17.cloned.1.call-done = bf16[2048,1024]{0,1:T(8,128)(2,1)} async-done(((bf16[512,1024]{0,1:T(8,128)(2,1)}), bf16[2048,1024]{0,1:T(8,128)(2,1)}) %all-gather.17.cloned.1.call-update) | async-done | bytes 4194320 | tf_op jit(solution)/shard_map/all_gather | solution.py:84
  466.8 6.5 %copy.24 = bf16[2048,1024]{1,0:T(8,128)(2,1)} copy(bf16[2048,1024]{0,1:T(8,128)(2,1)} %all-gather.17.cloned.1.call-done) | data formatting | bytes 8388608
  (14 shorter events, 0.0 us)
Async XLA Ops:
  7.2 56.9 %copy-start = (bf16[1536,1024]{1,0:T(8,128)(2,1)S(1)}, bf16[1536,1024]{1,0:T(8,128)(2,1)}, u32[]{:S(2)}) copy-start(bf16[1536,1024]{1,0:T(8,128)(2,1)} %param.12) | copy-start | bytes 9437188
  7.2 50.8 %all-gather.7.cloned.1.call-start = ((), (), s32[]{:S(2)}) async-start(), calls=%async_computation.2 | async-start | bytes 2621440 | tf_op jit(solution)/shard_map/all_gather | solution.py:45
  7.9 96.1 %all-gather.11.cloned.1.call-start = ((), (), s32[]{:S(2)}) async-start(), calls=%async_computation.5 | async-start | bytes 2621440 | tf_op jit(solution)/shard_map/all_gather | solution.py:46
  8.7 124.4 %reduce-scatter.3.cloned.1.call-start = ((), (), s32[]{:S(2)}) async-start(), calls=%async_computation.3 | async-start | bytes 1310720 | tf_op jit(solution)/shard_map/reduce_scatter | solution.py:53
  68.9 41.3 %copy-start.2 = (bf16[1536,1024]{1,0:T(8,128)(2,1)S(1)}, bf16[1536,1024]{1,0:T(8,128)(2,1)}, u32[]{:S(2)}) copy-start(bf16[1536,1024]{1,0:T(8,128)(2,1)} %param.13) | copy-start | bytes 9437188
  68.9 92.7 %reduce-scatter.5.cloned.1.call-start = ((), (), s32[]{:S(2)}) async-start(), calls=%async_computation.6 | async-start | bytes 1310720 | tf_op jit(solution)/shard_map/reduce_scatter | solution.py:56
  115.0 96.7 %copy-start.6 = (f32[128,1024]{1,0:T(8,128)S(1)}, f32[128,1024]{1,0:T(8,128)}, u32[]{:S(2)}) copy-start(f32[128,1024]{1,0:T(8,128)} %param.19) | copy-start | bytes 1572868
  115.0 96.6 %copy-start.7 = (f32[128,1024]{1,0:T(8,128)S(1)}, f32[128,1024]{1,0:T(8,128)}, u32[]{:S(2)}) copy-start(f32[128,1024]{1,0:T(8,128)} %param.17) | copy-start | bytes 1572868
  115.0 93.4 %all-reduce.4.cloned.1.call-start = ((), (), s32[]{:S(2)}) async-start(), calls=%async_computation.10 | async-start | bytes 1048576 | tf_op jit(solution)/shard_map/psum | solution.py:61
  161.6 96.0 %all-gather.9.cloned.1.call-start = ((), (), s32[]{:S(2)}) async-start(), calls=%async_computation.4 | async-start | bytes 2621440 | tf_op jit(solution)/shard_map/all_gather | solution.py:73
  208.4 3.3 copy-start.8
  211.5 2.2 copy-start.5
  211.6 92.6 %all-gather.13.cloned.1.call-start = ((), (), s32[]{:S(2)}) async-start(), calls=%async_computation.7 | async-start | bytes 2621440 | tf_op jit(solution)/shard_map/all_gather | solution.py:74
  213.6 44.1 %copy-start.3 = (bf16[512,512]{1,0:T(8,128)(2,1)S(1)}, bf16[512,512]{1,0:T(8,128)(2,1)}, u32[]{:S(2)}) copy-start(bf16[512,512]{1,0:T(8,128)(2,1)} %param.14) | copy-start | bytes 1572868
  213.6 172.4 %all-gather.15.cloned.1.call-start = ((), (), s32[]{:S(2)}) async-start(), calls=%async_computation.8 | async-start | bytes 5242880 | tf_op jit(solution)/shard_map/all_gather | solution.py:83
  264.3 39.9 %copy-start.4 = (bf16[512,512]{1,0:T(8,128)(2,1)S(1)}, bf16[512,512]{1,0:T(8,128)(2,1)}, u32[]{:S(2)}) copy-start(bf16[512,512]{1,0:T(8,128)(2,1)} %param.15) | copy-start | bytes 1572868
  264.3 202.4 %all-gather.17.cloned.1.call-start = ((), (), s32[]{:S(2)}) async-start(), calls=%async_computation.9 | async-start | bytes 5242880 | tf_op jit(solution)/shard_map/all_gather | solution.py:84
  466.8 6.5 %copy-start.1 = (bf16[1536,1024]{1,0:T(8,128)(2,1)S(1)}, bf16[1536,1024]{1,0:T(8,128)(2,1)}, u32[]{:S(2)}) copy-start(bf16[1536,1024]{1,0:T(8,128)(2,1)} %param.12) | copy-start | bytes 9437188
Sparse Core Ops, SparseCore 0:
  9.6 48.3 all-gather.6
  59.5 44.4 all-gather.10
  106.9 26.0 reduce-scatter.2
  135.7 25.7 reduce-scatter.4
  164.4 43.9 all-reduce.3
  211.7 45.8 all-gather.8
  259.8 44.4 all-gather.12
  306.3 79.5 all-gather.14
  387.5 79.2 all-gather.16
where the time goes:
time: 480 us
  waiting for transfers between devices  383 us (80%)
  matrix products  35.9 us (7%)
  local copies, waits for them, and re-layouts  22.7 us (5%)
  blocking collectives  17.6 us (4%)
  between operations  15.3 us (3%)
  other arithmetic  5.05 us (1%)
    all_gather x1, waiting for transfers between devices, body(): lax.all_gather(copy_gate, 'fs', axis=0, tiled=True)  74.4 us
    all_gather x1, waiting for transfers between devices, body(): lax.all_gather(copy_rec, 'fs', axis=0, tiled=True)  69.5 us
    all_gather x1, waiting for transfers between devices, body(): lax.all_gather(factor_rec, 'fs', axis=0, tiled=True)  49.3 us
    psum x1, waiting for transfers between devices, body(): lax.psum(low_rec.astype(jnp.bfloat16), 'rep').astype(jnp.float32)  46.7 us
    all_gather x1, waiting for transfers between devices, body(): lax.all_gather(direc_gate, 'fs', axis=0, tiled=True)  36.1 us
    all_gather x1, waiting for transfers between devices, body(): lax.all_gather(factor_gate, 'fs', axis=0, tiled=True)  35.1 us
    reduce_scatter x1, waiting for transfers between devices, body(): lax.psum_scatter(part_gate.astype(jnp.bfloat16), 'fs', scatter_dimension=...  28.6 us
    all_gather x1, waiting for transfers between devices, body(): lax.all_gather(direc_rec, 'fs', axis=0, tiled=True)  23.8 us
  transfers between devices with their start and end apart: 9, of which 9 were waited for; matrix products, arithmetic and copies ran while one was open for 11% of the time, Pallas kernels for 0%

commit v1 on v0

--- a/solution.py
+++ b/solution.py
@@ -1,7 +1,9 @@
+import functools
 import jax
 import jax.numpy as jnp
 from jax import lax
 from jax.sharding import PartitionSpec as P
+from jax.lax import all_gather
 
 DR = 2048
 RANK = 512
@@ -9,6 +11,15 @@
 beta_second = 0.9
 scale_floor = 0.25
 step_rate = 0.01
+
+
+def put_limits(page, named_axis):
+    carry_out = all_gather(page, axis_name=named_axis)
+    w1 = jnp.sum(carry_out, axis=0)
+    return w1
+
+
+reach_strings = functools.partial(put_limits, named_axis="rep")
 
 
 def split_product(projected, cotan):
@@ -58,7 +69,7 @@
         ).astype(jnp.float32),
     )
     low_rec, low_gate = (
-        lax.psum(low_rec.astype(jnp.bfloat16), "rep").astype(jnp.float32),
+        reach_strings(low_rec.astype(jnp.bfloat16)).astype(jnp.float32),
         lax.psum(low_gate.astype(jnp.bfloat16), "rep").astype(jnp.float32),
     )
     first_r, second_r, direc_rec = moments(low_rec, first_rec, second_rec)

time: 480 us -> 505 us (1.052)
  waiting for transfers between devices: 383 us -> 404 us
    all_gather x0 -> x1, waiting for transfers between devices: none -> 25.1 us  [put_limits(): carry_out = all_gather(page, axis_name=named_axis)]
    all_gather x1, waiting for transfers between devices: 35.1 us -> 49.3 us  [body(): lax.all_gather(factor_gate, 'fs', axis=0, tiled=True)]
    all_gather x1, waiting for transfers between devices: 49.3 us -> 35.1 us  [body(): lax.all_gather(factor_rec, 'fs', axis=0, tiled=True)]
    all_gather x1, waiting for transfers between devices: 36.1 us -> 23 us  [body(): lax.all_gather(direc_gate, 'fs', axis=0, tiled=True)]
    all_gather x1, waiting for transfers between devices: 23.8 us -> 36 us  [body(): lax.all_gather(direc_rec, 'fs', axis=0, tiled=True)]
    reduce_scatter x1, waiting for transfers between devices: 28.6 us -> 18 us  [body(): lax.psum_scatter(part_gate.astype(jnp.bfloat16), 'fs', scatter_dimension=...]
    reduce_scatter x1, waiting for transfers between devices: 18 us -> 28.5 us  [body(): lax.psum_scatter(part_rec.astype(jnp.bfloat16), 'fs', scatter_dimension=0...]
    all_gather x1, waiting for transfers between devices: 74.4 us -> 68.9 us  [body(): lax.all_gather(copy_gate, 'fs', axis=0, tiled=True)]
  transfers between devices with their start and end apart: 9 -> 10, of which waited for: 9 -> 10; matrix products, arithmetic and copies ran while one was open for 11% -> 12% of each run, Pallas kernels for 0% -> 0%
where the time goes in v1:
time: 505 us
  waiting for transfers between devices  404 us (80%)
  matrix products  35.9 us (7%)
  local copies, waits for them, and re-layouts  22.7 us (4%)
  blocking collectives  18.1 us (4%)
  between operations  15.6 us (3%)
  other arithmetic  7.57 us (1%)
    all_gather x1, waiting for transfers between devices, body(): lax.all_gather(copy_rec, 'fs', axis=0, tiled=True)  74.9 us
    all_gather x1, waiting for transfers between devices, body(): lax.all_gather(copy_gate, 'fs', axis=0, tiled=True)  68.9 us
    all_gather x1, waiting for transfers between devices, body(): lax.all_gather(factor_gate, 'fs', axis=0, tiled=True)  49.3 us
    psum x1, waiting for transfers between devices, body(): lax.psum(low_gate.astype(jnp.bfloat16), 'rep').astype(jnp.float32)  44.3 us
    all_gather x1, waiting for transfers between devices, body(): lax.all_gather(direc_rec, 'fs', axis=0, tiled=True)  36 us
    all_gather x1, waiting for transfers between devices, body(): lax.all_gather(factor_rec, 'fs', axis=0, tiled=True)  35.1 us
    reduce_scatter x1, waiting for transfers between devices, body(): lax.psum_scatter(part_rec.astype(jnp.bfloat16), 'fs', scatter_dimension=0...  28.5 us
    all_gather x1, waiting for transfers between devices, put_limits(): carry_out = all_gather(page, axis_name=named_axis)  25.1 us
  transfers between devices with their start and end apart: 10, of which 10 were waited for; matrix products, arithmetic and copies ran while one was open for 12% of the time, Pallas kernels for 0%

profile of v1, /device:TPU:0, one launch (start us, length us, event | category | flops | bytes accessed | tf_op | source)
XLA Modules:
  0.0 504.6 jit_solution(17767868257868395551)
XLA Ops:
  7.2 0.0 all-gather.13.cloned.1.call-start
  7.2 0.7 all-gather.13.cloned.1.call-update
  7.9 0.0 all-gather.9.cloned.1.call-start
  8.0 0.7 all-gather.9.cloned.1.call-update
  8.7 0.0 reduce-scatter.5.cloned.1.call-start
  8.7 49.3 %all-gather.13.cloned.1.call-done = bf16[2048,512]{1,0:T(8,128)(2,1)} async-done(((bf16[512,512]{1,0:T(8,128)(2,1)}), bf16[2048,512]{1,0:T(8,128)(2,1)}) %all-gather.13.cloned.1.call-update) | async-done | bytes 2097168 | tf_op jit(solution)/shard_map/all_gather | solution.py:57
  58.0 6.1 %fusion.15 = f32[1536,512]{1,0:T(8,128)S(1)} fusion(bf16[1536,2048]{1,0:T(8,128)(2,1)} %param.11, bf16[2048,512]{1,0:T(8,128)(2,1)} %all-gather.13.cloned.1.call-done), kind=kOutput, calls=%fused_computation.27 | convolution fusion | flops 3221225472 | bytes 11534336 | tf_op jit(solution)/shard_map/dot_general | solution.py:60
  64.1 1.9 fusion.1
  66.0 2.9 add_convert_fusion
  68.9 0.0 reduce-scatter.5.cloned.1.call-update
  68.9 0.0 reduce-scatter.3.cloned.1.call-start
  69.0 35.1 %all-gather.9.cloned.1.call-done = bf16[2048,512]{1,0:T(8,128)(2,1)} async-done(((bf16[512,512]{1,0:T(8,128)(2,1)}), bf16[2048,512]{1,0:T(8,128)(2,1)}) %all-gather.9.cloned.1.call-update) | async-done | bytes 2097168 | tf_op jit(solution)/shard_map/all_gather | solution.py:56
  104.0 6.1 %fusion.14 = f32[1536,512]{1,0:T(8,128)S(1)} fusion(bf16[1536,2048]{1,0:T(8,128)(2,1)} %param.11, bf16[2048,512]{1,0:T(8,128)(2,1)} %all-gather.9.cloned.1.call-done), kind=kOutput, calls=%fused_computation.26 | convolution fusion | flops 3221225472 | bytes 11534336 | tf_op jit(solution)/shard_map/dot_general | solution.py:59
  110.2 1.9 fusion
  112.1 2.9 add_convert_fusion.1
  114.9 0.0 reduce-scatter.3.cloned.1.call-update
  115.0 0.0 all-reduce.3.cloned.1.call-start
  115.0 18.0 %reduce-scatter.5.cloned.1.call-done = bf16[128,1024]{1,0:T(8,128)(2,1)} async-done(((bf16[512,1024]{1,0:T(8,128)(2,1)}), bf16[128,1024]{1,0:T(8,128)(2,1)}) %reduce-scatter.5.cloned.1.call-update) | async-done | bytes 262160 | tf_op jit(solution)/shard_map/reduce_scatter | solution.py:67
  133.0 0.0 all-reduce.3.cloned.1.call-update
  133.0 0.0 all-gather.21.cloned.1.call-start
  133.1 28.5 %reduce-scatter.3.cloned.1.call-done = bf16[128,1024]{1,0:T(8,128)(2,1)} async-done(((bf16[512,1024]{1,0:T(8,128)(2,1)}), bf16[128,1024]{1,0:T(8,128)(2,1)}) %reduce-scatter.3.cloned.1.call-update) | async-done | bytes 262160 | tf_op jit(solution)/shard_map/reduce_scatter | solution.py:64
  161.6 0.0 all-gather.21.cloned.1.call-update
  161.6 0.0 all-gather.15.cloned.1.call-start
  161.7 44.3 %all-reduce.3.cloned.1.call-done = bf16[128,1024]{1,0:T(8,128)(2,1)} async-done(((bf16[128,1024]{1,0:T(8,128)(2,1)}), bf16[128,1024]{1,0:T(8,128)(2,1)}) %all-reduce.3.cloned.1.call-update) | async-done | bytes 262160 | tf_op jit(solution)/shard_map/psum | solution.py:73
  206.0 3.1 multiply_reduce_fusion
  209.1 0.0 all-gather.15.cloned.1.call-update
  209.1 0.0 all-gather.11.cloned.1.call-start
  209.1 25.1 %all-gather.21.cloned.1.call-done = bf16[512,1024]{1,0:T(8,128)(2,1)} async-done(((bf16[128,1024]{1,0:T(8,128)(2,1)}), bf16[512,1024]{1,0:T(8,128)(2,1)}) %all-gather.21.cloned.1.call-update) | async-done | bytes 1048592 | tf_op jit(solution)/shard_map/all_gather | solution.py:17
  234.2 1.6 reduce_sum.30
  235.8 2.9 multiply_reduce_fusion.1
  238.7 0.0 all-gather.11.cloned.1.call-update
  238.7 0.0 all-gather.19.cloned.1.call-start
  238.8 1.8 copy.20
  240.6 18.1 %all-reduce = (f32[]{:T(128)}, f32[]{:T(128)}) all-reduce(f32[]{:T(128)} %get-tuple-element.22, f32[]{:T(128)} %get-tuple-element.18), channel_id=1, replica_groups=mesh['fs'=4,'rep'=4,'tp'=2] {'fs','tp'}, use_global_device_ids=true, to_apply=%region_3.0 | all-reduce | flops 2 | bytes 16 | tf_op jit(solution)/shard_map/psum | solution.py:77
  259.3 23.0 %all-gather.15.cloned.1.call-done = f32[512,1024]{1,0:T(8,128)} async-done(((f32[128,1024]{1,0:T(8,128)}), f32[512,1024]{1,0:T(8,128)}) %all-gather.15.cloned.1.call-update) | async-done | bytes 2097168 | tf_op jit(solution)/shard_map/all_gather | solution.py:85
  282.2 6.8 %subtract_convert_fusion.2 = (bf16[512,1024]{0,1:T(8,128)(2,1)}, f32[512,1024]{0,1:T(8,128)S(1)}) fusion(f32[512,1024]{0,1:T(8,128)} %copy.20, f32[]{:T(128)S(6)} %sqrt.15, f32[512,1024]{1,0:T(8,128)} %all-gather.15.cloned.1.call-done, bf16[512,512]{1,0:T(8,128)(2,1)S(1)} %copy-done.3), kind=kOutput, calls=%fused_computation.2 | convolution fusion | flops 3223322624 | bytes 7864324 | tf_op jit(solution)/shard_map/dot_general | solution.py:88
  289.0 0.0 all-gather.19.cloned.1.call-update
  289.0 0.0 all-gather.17.cloned.1.call-start
  289.1 3.0 copy.19
  292.8 36.0 %all-gather.11.cloned.1.call-done = f32[512,1024]{1,0:T(8,128)} async-done(((f32[128,1024]{1,0:T(8,128)}), f32[512,1024]{1,0:T(8,128)}) %all-gather.11.cloned.1.call-update) | async-done | bytes 2097168 | tf_op jit(solution)/shard_map/all_gather | solution.py:84
  328.8 7.3 %subtract_convert_fusion.3 = (bf16[512,1024]{0,1:T(8,128)(2,1)}, f32[512,1024]{0,1:T(8,128)}) fusion(f32[512,1024]{0,1:T(8,128)} %copy.19, f32[]{:T(128)S(6)} %sqrt.13, f32[512,1024]{1,0:T(8,128)} %all-gather.11.cloned.1.call-done, bf16[512,512]{1,0:T(8,128)(2,1)S(1)} %copy-done.4), kind=kOutput, calls=%fused_computation.3 | convolution fusion | flops 3223322624 | bytes 7864324 | tf_op jit(solution)/shard_map/dot_general | solution.py:87
  336.2 0.0 all-gather.17.cloned.1.call-update
  336.2 1.8 copy.22
  338.0 3.0 copy.21
  341.1 68.9 %all-gather.19.cloned.1.call-done = bf16[2048,1024]{0,1:T(8,128)(2,1)} async-done(((bf16[512,1024]{0,1:T(8,128)(2,1)}), bf16[2048,1024]{0,1:T(8,128)(2,1)}) %all-gather.19.cloned.1.call-update) | async-done | bytes 4194320 | tf_op jit(solution)/shard_map/all_gather | solution.py:95
  410.0 6.4 %copy.24 = bf16[2048,1024]{1,0:T(8,128)(2,1)} copy(bf16[2048,1024]{0,1:T(8,128)(2,1)} %all-gather.19.cloned.1.call-done) | data formatting | bytes 8388608
  416.4 74.9 %all-gather.17.cloned.1.call-done = bf16[2048,1024]{0,1:T(8,128)(2,1)} async-done(((bf16[512,1024]{0,1:T(8,128)(2,1)}), bf16[2048,1024]{0,1:T(8,128)(2,1)}) %all-gather.17.cloned.1.call-update) | async-done | bytes 4194320 | tf_op jit(solution)/shard_map/all_gather | solution.py:94
  491.2 6.5 %copy.23 = bf16[2048,1024]{1,0:T(8,128)(2,1)} copy(bf16[2048,1024]{0,1:T(8,128)(2,1)} %all-gather.17.cloned.1.call-done) | data formatting | bytes 8388608
  (14 shorter events, 0.0 us)
Async XLA Ops:
  7.2 56.9 %copy-start = (bf16[1536,1024]{1,0:T(8,128)(2,1)S(1)}, bf16[1536,1024]{1,0:T(8,128)(2,1)}, u32[]{:S(2)}) copy-start(bf16[1536,1024]{1,0:T(8,128)(2,1)} %param.13) | copy-start | bytes 9437188
  7.2 50.8 %all-gather.13.cloned.1.call-start = ((), (), s32[]{:S(2)}) async-start(), calls=%async_computation.5 | async-start | bytes 2621440 | tf_op jit(solution)/shard_map/all_gather | solution.py:57
  7.9 96.1 %all-gather.9.cloned.1.call-start = ((), (), s32[]{:S(2)}) async-start(), calls=%async_computation.2 | async-start | bytes 2621440 | tf_op jit(solution)/shard_map/all_gather | solution.py:56
  8.7 124.4 %reduce-scatter.5.cloned.1.call-start = ((), (), s32[]{:S(2)}) async-start(), calls=%async_computation.6 | async-start | bytes 1310720 | tf_op jit(solution)/shard_map/reduce_scatter | solution.py:67
  68.9 41.3 %copy-start.2 = (bf16[1536,1024]{1,0:T(8,128)(2,1)S(1)}, bf16[1536,1024]{1,0:T(8,128)(2,1)}, u32[]{:S(2)}) copy-start(bf16[1536,1024]{1,0:T(8,128)(2,1)} %param.12) | copy-start | bytes 9437188
  68.9 92.7 %reduce-scatter.3.cloned.1.call-start = ((), (), s32[]{:S(2)}) async-start(), calls=%async_computation.3 | async-start | bytes 1310720 | tf_op jit(solution)/shard_map/reduce_scatter | solution.py:64
  115.0 91.0 %all-reduce.3.cloned.1.call-start = ((), (), s32[]{:S(2)}) async-start(), calls=%async_computation.7 | async-start | bytes 524288 | tf_op jit(solution)/shard_map/psum | solution.py:73
  133.0 101.1 %all-gather.21.cloned.1.call-start = ((), (), s32[]{:S(2)}) async-start(), calls=%async_computation.11 | async-start | bytes 1310720 | tf_op jit(solution)/shard_map/all_gather | solution.py:17
  161.6 74.2 %copy-start.6 = (f32[128,1024]{1,0:T(8,128)S(1)}, f32[128,1024]{1,0:T(8,128)}, u32[]{:S(2)}) copy-start(f32[128,1024]{1,0:T(8,128)} %param.18) | copy-start | bytes 1572868
  161.6 120.6 %all-gather.15.cloned.1.call-start = ((), (), s32[]{:S(2)}) async-start(), calls=%async_computation.8 | async-start | bytes 2621440 | tf_op jit(solution)/shard_map/all_gather | solution.py:85
  209.1 119.8 %all-gather.11.cloned.1.call-start = ((), (), s32[]{:S(2)}) async-start(), calls=%async_computation.4 | async-start | bytes 2621440 | tf_op jit(solution)/shard_map/all_gather | solution.py:84
  234.2 4.6 copy-start.5
  238.7 43.5 %copy-start.3 = (bf16[512,512]{1,0:T(8,128)(2,1)S(1)}, bf16[512,512]{1,0:T(8,128)(2,1)}, u32[]{:S(2)}) copy-start(bf16[512,512]{1,0:T(8,128)(2,1)} %param.15) | copy-start | bytes 1572868
  238.7 171.3 %all-gather.19.cloned.1.call-start = ((), (), s32[]{:S(2)}) async-start(), calls=%async_computation.10 | async-start | bytes 5242880 | tf_op jit(solution)/shard_map/all_gather | solution.py:95
  289.0 39.8 %copy-start.4 = (bf16[512,512]{1,0:T(8,128)(2,1)S(1)}, bf16[512,512]{1,0:T(8,128)(2,1)}, u32[]{:S(2)}) copy-start(bf16[512,512]{1,0:T(8,128)(2,1)} %param.14) | copy-start | bytes 1572868
  289.0 202.2 %all-gather.17.cloned.1.call-start = ((), (), s32[]{:S(2)}) async-start(), calls=%async_computation.9 | async-start | bytes 5242880 | tf_op jit(solution)/shard_map/all_gather | solution.py:94
  491.2 6.5 %copy-start.1 = (bf16[1536,1024]{1,0:T(8,128)(2,1)S(1)}, bf16[1536,1024]{1,0:T(8,128)(2,1)}, u32[]{:S(2)}) copy-start(bf16[1536,1024]{1,0:T(8,128)(2,1)} %param.13) | copy-start | bytes 9437188
Sparse Core Ops, SparseCore 0:
  9.6 48.3 all-gather.12
  59.5 44.4 all-gather.8
  106.9 26.0 reduce-scatter.4
  135.7 25.7 reduce-scatter.2
  164.4 41.5 all-reduce.2
  207.7 26.4 all-gather.20
  236.3 45.8 all-gather.14
  284.4 44.4 all-gather.10
  330.4 79.5 all-gather.18
  412.0 79.2 all-gather.16
